TPU v7x, 32 devices: a whole 2x2x4 slice. The times are simulated.
32 devices in a mesh: fs: 16 (over z, y, x), tp: 2 (over core).
Axes of the slice: x: 2, y: 2, z: 4, core: 2. Of those that a mesh axis runs over, the one named last changes fastest.
Arguments:
- normed: bfloat16 [16384, 2048], P('fs'), may hold values from -6 to 6
- key_cot: bfloat16 [16384, 1024], P('fs', 'tp'), may hold values from -130 to 130
- value_cot: bfloat16 [16384, 2048], P('fs', 'tp'), may hold values from -130 to 130
- basis: bfloat16 [2048, 256], P('fs'), may hold values from -3.535534 to 3.535534
- master_key: float32 [2048, 1024], P('fs', 'tp'), may hold values from -3 to 3
- master_value: float32 [2048, 2048], P('fs', 'tp'), may hold values from -3 to 3
- first_key: float32 [256, 1024], P('fs', 'tp'), may hold values from -3 to 3
- second_key: float32 [256, 1024], P('fs', 'tp'), may hold values from 0.05 to 2
- first_value: float32 [256, 2048], P('fs', 'tp'), may hold values from -3 to 3
- second_value: float32 [256, 2048], P('fs', 'tp'), may hold values from 0.05 to 2
Outputs:
- step_key: float32 [2048, 1024], P('fs', 'tp')
- step_value: float32 [2048, 2048], P('fs', 'tp')
- new_master_key: float32 [2048, 1024], P('fs', 'tp')
- new_master_value: float32 [2048, 2048], P('fs', 'tp')
- copy_key: bfloat16 [2048, 1024], P(None, 'tp')
- copy_value: bfloat16 [2048, 2048], P(None, 'tp')
- new_first_key: float32 [256, 1024], P('fs', 'tp')
- new_second_key: float32 [256, 1024], P('fs', 'tp')
- new_first_value: float32 [256, 2048], P('fs', 'tp')
- new_second_value: float32 [256, 2048], P('fs', 'tp')
All inputs are finite; a program needn't handle non-finite values.
Results may differ from a plain program's by a relative error of at most 0.0055.
Values may be sent and summed in bfloat16 or wider, within the bound.
A program may use at most 64 MiB of HBM per device.

v0:
```python
import jax
import jax.numpy as jnp
from jax import lax
from jax.sharding import PartitionSpec as P

DK = 1024
DV = 2048
R = 256
learn_rate = 0.05
beta_first = 0.9
beta_second = 0.9
epsilon = 1e-08
norm_eps = 1e-06


def on_device(
    normed,
    key_cot,
    value_cot,
    basis,
    master_key,
    master_value,
    first_key,
    second_key,
    first_value,
    second_value,
):
    key_cols = key_cot.shape[1]
    cotangents = jnp.concatenate([key_cot, value_cot], axis=1)
    projected = jnp.dot(
        normed, lax.all_gather(basis, "fs", axis=0, tiled=True), preferred_element_type=jnp.float32
    )
    upper_part = projected.astype(jnp.bfloat16)
    lower_part = (projected - upper_part.astype(jnp.float32)).astype(jnp.bfloat16)
    partial_value = lax.dot_general(
        upper_part, cotangents, (((0,), (0,)), ((), ())), preferred_element_type=jnp.float32
    )
    partial_value = partial_value + lax.dot_general(
        lower_part, cotangents, (((0,), (0,)), ((), ())), preferred_element_type=jnp.float32
    )
    rank_rows = first_key.shape[0]
    summed = lax.psum(partial_value, "fs")
    squares = lax.psum(jnp.sum(summed * summed), "tp")
    own_rows = lax.dynamic_slice_in_dim(summed, lax.axis_index("fs") * rank_rows, rank_rows, 0)
    root_mean = jnp.sqrt(squares / (R * (DK + DV)) + norm_eps)
    grad_scale = 1.0 / root_mean
    first_moment = jnp.concatenate([first_key, first_value], axis=1)
    second_moment = jnp.concatenate([second_key, second_value], axis=1)
    scaled = own_rows * grad_scale
    new_first = beta_first * first_moment + (1.0 - beta_first) * scaled
    new_second = beta_second * second_moment + (1.0 - beta_second) * scaled * scaled
    direction = (new_first / (jnp.sqrt(new_second) + epsilon)).astype(jnp.bfloat16)
    all_directions = lax.all_gather(direction, "fs", axis=0, tiled=True)
    update_step = jnp.dot(basis, all_directions, preferred_element_type=jnp.float32)
    master = jnp.concatenate([master_key, master_value], axis=1)
    new_master = master - learn_rate * update_step
    half_copy = new_master.astype(jnp.bfloat16)
    copy_key, copy_value = (
        lax.all_gather(half_copy[:, :key_cols], "fs", axis=0, tiled=True),
        lax.all_gather(half_copy[:, key_cols:], "fs", axis=0, tiled=True),
    )
    return (
        update_step[:, :key_cols],
        update_step[:, key_cols:],
        new_master[:, :key_cols],
        new_master[:, key_cols:],
        copy_key,
        copy_value,
        new_first[:, :key_cols],
        new_second[:, :key_cols],
        new_first[:, key_cols:],
        new_second[:, key_cols:],
    )


def solution(mesh):
    placed = (
        P("fs", None),
        P("fs", "tp"),
        P("fs", "tp"),
        P("fs", None),
        P("fs", "tp"),
        P("fs", "tp"),
        P("fs", "tp"),
        P("fs", "tp"),
        P("fs", "tp"),
        P("fs", "tp"),
    )
    return jax.shard_map(
        on_device,
        mesh=mesh,
        in_specs=placed,
        out_specs=(
            P("fs", "tp"),
            P("fs", "tp"),
            P("fs", "tp"),
            P("fs", "tp"),
            P(None, "tp"),
            P(None, "tp"),
            P("fs", "tp"),
            P("fs", "tp"),
            P("fs", "tp"),
            P("fs", "tp"),
        ),
        check_vma=False,
    )
```

profile of v0, /device:TPU:0, one launch (start us, length us, event | category | flops | bytes accessed | tf_op | source)
XLA Modules:
  0.0 406.0 jit_solution(744935510458757411)
XLA Ops:
  7.2 0.7 all-gather.4.cloned.1.call-update
  8.0 1.4 constant_dynamic-update-slice_fusion.1
  10.0 58.5 %all-gather.4.cloned.1.call-done = bf16[2048,256]{1,0:T(8,128)(2,1)} async-done(((bf16[128,256]{1,0:T(8,128)(2,1)}), bf16[2048,256]{1,0:T(8,128)(2,1)}) %all-gather.4.cloned.1.call-update) | async-done | bytes 1048592 | tf_op jit(solution)/shard_map/all_gather | solution.py:31
  68.6 3.7 fusion.6
  72.3 1.0 fusion.1
  73.4 2.2 convolution_add_fusion
  75.8 1.2 copy.21
  77.0 115.1 %all-reduce.2.cloned.1.call-done = f32[256,1536]{1,0:T(8,128)} async-done(((f32[256,1536]{1,0:T(8,128)}), f32[256,1536]{1,0:T(8,128)}) %all-reduce.2.cloned.1.call-update) | async-done | bytes 1572880 | tf_op jit(solution)/shard_map/psum | solution.py:42
  192.1 2.4 multiply_reduce_fusion
  194.5 3.1 psum.15
  198.3 1.0 divide_convert_fusion
  199.3 43.7 %all_gather.13 = bf16[256,1536]{1,0:T(8,128)(2,1)S(1)} all-gather(bf16[16,1536]{1,0:T(8,128)(2,1)S(1)} %get-tuple-element.22), channel_id=1, replica_groups=mesh['fs'=16,'tp'=2] {'fs'}, dimensions={0}, use_global_device_ids=true | all-gather | bytes 835584 | tf_op jit(solution)/shard_map/all_gather | solution.py:53
  243.4 0.7 slice.44
  244.1 0.7 slice.45
  245.5 0.6 slice.49
  246.7 0.6 slice.48
  247.5 1.0 copy.25
  248.5 0.8 copy.24
  249.4 1.0 copy.23
  250.3 0.8 copy.22
  251.2 51.9 %all-gather.6.cloned.1.call-done = bf16[2048,512]{0,1:T(8,128)(2,1)} async-done(((bf16[128,512]{0,1:T(8,128)(2,1)}), bf16[2048,512]{0,1:T(8,128)(2,1)}) %all-gather.6.cloned.1.call-update) | async-done | bytes 2097168 | tf_op jit(solution)/shard_map/all_gather | solution.py:59
  303.0 3.9 copy.26
  307.0 86.1 %all-gather.8.cloned.1.call-done = bf16[2048,1024]{0,1:T(8,128)(2,1)} async-done(((bf16[128,1024]{0,1:T(8,128)(2,1)}), bf16[2048,1024]{0,1:T(8,128)(2,1)}) %all-gather.8.cloned.1.call-update) | async-done | bytes 4194320 | tf_op jit(solution)/shard_map/all_gather | solution.py:60
  393.1 6.4 %copy.27 = bf16[2048,1024]{1,0:T(8,128)(2,1)} copy(bf16[2048,1024]{0,1:T(8,128)(2,1)} %all-gather.8.cloned.1.call-done) | data formatting | bytes 8388608
  (30 shorter events, 2.7 us)
Async XLA Ops:
  7.2 61.4 %all-gather.4.cloned.1.call-start = ((), (), s32[]{:S(2)}) async-start(), calls=%async_computation | async-start | bytes 1114112 | tf_op jit(solution)/shard_map/all_gather | solution.py:31
  7.9 184.2 %all-reduce.2.cloned.1.call-start = ((), (), s32[]{:S(2)}) async-start(), calls=%async_computation.1 | async-start | bytes 3145728 | tf_op jit(solution)/shard_map/psum | solution.py:42
  8.0 1.9 copy-start
  73.4 2.3 copy-start.2
  75.5 122.7 %copy-start.3 = (f32[16,1024]{1,0:T(8,128)S(1)}, f32[16,1024]{1,0:T(8,128)}, u32[]{:S(2)}) copy-start(f32[16,1024]{1,0:T(8,128)} %param.19) | copy-start | bytes 196612
  75.5 122.8 %copy-start.4 = (f32[16,1024]{1,0:T(8,128)S(1)}, f32[16,1024]{1,0:T(8,128)}, u32[]{:S(2)}) copy-start(f32[16,1024]{1,0:T(8,128)} %param.18) | copy-start | bytes 196612
  75.5 122.8 %copy-start.5 = (f32[16,512]{1,0:T(8,128)S(1)}, f32[16,512]{1,0:T(8,128)}, u32[]{:S(2)}) copy-start(f32[16,512]{1,0:T(8,128)} %param.17) | copy-start | bytes 98308
  75.5 122.8 %copy-start.6 = (f32[16,512]{1,0:T(8,128)S(1)}, f32[16,512]{1,0:T(8,128)}, u32[]{:S(2)}) copy-start(f32[16,512]{1,0:T(8,128)} %param.16) | copy-start | bytes 98308
  75.5 167.4 %copy-start.1 = (bf16[128,256]{1,0:T(8,128)(2,1)S(1)}, bf16[128,256]{1,0:T(8,128)(2,1)}, u32[]{:S(2)}) copy-start(bf16[128,256]{1,0:T(8,128)(2,1)} %param.13) | copy-start | bytes 196612
  75.6 227.5 %all-gather.6.cloned.1.call-start = ((), (), s32[]{:S(2)}) async-start(), calls=%async_computation.2 | async-start | bytes 2228224 | tf_op jit(solution)/shard_map/all_gather | solution.py:59
  244.1 149.0 %all-gather.8.cloned.1.call-start = ((), (), s32[]{:S(2)}) async-start(), calls=%async_computation.3 | async-start | bytes 4456448 | tf_op jit(solution)/shard_map/all_gather | solution.py:60
Sparse Core Ops, SparseCore 0:
  10.7 57.7 all-gather.3
  75.7 116.3 all-reduce.1
  244.2 58.7 all-gather.5
  306.2 86.8 all-gather.7
where the time goes:
time: 406 us
  waiting for transfers between devices  312 us (77%)
  blocking collectives  46.8 us (12%)
  local copies, waits for them, and re-layouts  21.4 us (5%)
  between operations  14.6 us (4%)
  matrix products  7.34 us (2%)
    psum x1, waiting for transfers between devices, on_device(): summed = lax.psum(partial_value, 'fs')  115 us
    all_gather x1, waiting for transfers between devices, on_device(): lax.all_gather(half_copy[:, key_cols:], 'fs', axis=0, tiled=True)  86.1 us
    all_gather x1, waiting for transfers between devices, on_device(): lax.all_gather(basis, 'fs', axis=0, tiled=True)  58.5 us
    all_gather x1, waiting for transfers between devices, on_device(): lax.all_gather(half_copy[:, :key_cols], 'fs', axis=0, tiled=True)  51.9 us
    all_gather x1, blocking collectives, on_device(): all_directions = lax.all_gather(direction, 'fs', axis=0, tiled=True)  43.7 us
    unnamed x23, local copies, waits for them, and re-layouts  17.3 us
  transfers between devices with their start and end apart: 4, of which 4 were waited for; matrix products, arithmetic and copies ran while one was open for 3% of the time, Pallas kernels for 0%

commit v1 on v0

--- a/solution.py
+++ b/solution.py
@@ -39,7 +39,7 @@
         lower_part, cotangents, (((0,), (0,)), ((), ())), preferred_element_type=jnp.float32
     )
     rank_rows = first_key.shape[0]
-    summed = lax.psum(partial_value, "fs")
+    summed = jnp.sum(lax.all_gather(partial_value, "fs"), axis=0)
     squares = lax.psum(jnp.sum(summed * summed), "tp")
     own_rows = lax.dynamic_slice_in_dim(summed, lax.axis_index("fs") * rank_rows, rank_rows, 0)
     root_mean = jnp.sqrt(squares / (R * (DK + DV)) + norm_eps)

time: 406 us -> 566 us (1.39)
  waiting for transfers between devices: 312 us -> 466 us
  other arithmetic: 3.39 us -> 11 us
    all_gather x0 -> x1, waiting for transfers between devices: none -> 268 us  [on_device(): summed = jnp.sum(lax.all_gather(partial_value, 'fs'), axis=0)]
    psum x1 -> x0, waiting for transfers between devices: 115 us -> none  [on_device(): summed = lax.psum(partial_value, 'fs')]
    reduce_sum x0 -> x1, other arithmetic: none -> 9.93 us  [on_device(): summed = jnp.sum(lax.all_gather(partial_value, 'fs'), axis=0)]
  transfers between devices with their start and end apart: 4 -> 4, of which waited for: 4 -> 4; matrix products, arithmetic and copies ran while one was open for 3% -> 2% of each run, Pallas kernels for 0% -> 0%
where the time goes in v1:
time: 566 us
  waiting for transfers between devices  466 us (82%)
  blocking collectives  45.4 us (8%)
  local copies, waits for them, and re-layouts  21.4 us (4%)
  between operations  14.6 us (3%)
  other arithmetic  11 us (2%)
  matrix products  7.35 us (1%)
    all_gather x1, waiting for transfers between devices, on_device(): summed = jnp.sum(lax.all_gather(partial_value, 'fs'), axis=0)  268 us
    all_gather x1, waiting for transfers between devices, on_device(): lax.all_gather(half_copy[:, key_cols:], 'fs', axis=0, tiled=True)  86.1 us
    all_gather x1, waiting for transfers between devices, on_device(): lax.all_gather(basis, 'fs', axis=0, tiled=True)  58.5 us
    all_gather x1, waiting for transfers between devices, on_device(): lax.all_gather(half_copy[:, :key_cols], 'fs', axis=0, tiled=True)  52.2 us
    all_gather x1, blocking collectives, on_device(): all_directions = lax.all_gather(direction, 'fs', axis=0, tiled=True)  42.4 us
    unnamed x23, local copies, waits for them, and re-layouts  17.2 us
  transfers between devices with their start and end apart: 4, of which 4 were waited for; matrix products, arithmetic and copies ran while one was open for 2% of the time, Pallas kernels for 0%

profile of v1, /device:TPU:0, one launch (start us, length us, event | category | flops | bytes accessed | tf_op | source)
XLA Modules:
  0.0 565.7 jit_solution(10767465060162287686)
XLA Ops:
  7.2 0.7 all-gather.6.cloned.1.call-update
  8.0 1.4 constant_dynamic-update-slice_fusion.1
  10.0 58.5 %all-gather.6.cloned.1.call-done = bf16[2048,256]{1,0:T(8,128)(2,1)} async-done(((bf16[128,256]{1,0:T(8,128)(2,1)}), bf16[2048,256]{1,0:T(8,128)(2,1)}) %all-gather.6.cloned.1.call-update) | async-done | bytes 1048592 | tf_op jit(solution)/shard_map/all_gather | solution.py:31
  68.6 3.7 fusion.6
  72.3 1.0 fusion.1
  73.4 2.2 convolution_add_fusion
  75.6 1.2 copy.21
  77.0 268.1 %all-gather.12.cloned.1.call-done = f32[4096,1536]{1,0:T(8,128)} async-done(((f32[256,1536]{1,0:T(8,128)}), f32[4096,1536]{1,0:T(8,128)}) %all-gather.12.cloned.1.call-update) | async-done | bytes 25165840 | tf_op jit(solution)/shard_map/all_gather | solution.py:42
  345.1 9.9 %reduce_sum.18 = f32[256,1536]{1,0:T(8,128)S(1)} reduce(f32[16,256,1536]{2,1,0:T(8,128)} %bitcast.9, f32[]{:T(128)} %constant.3.clone.1), dimensions={0}, to_apply=%region_0.0 | reduce | flops 5898240 | bytes 26738692 | tf_op jit(solution)/shard_map/reduce_sum | solution.py:42
  355.0 1.0 multiply_reduce_fusion
  356.0 3.1 psum.7
  359.9 42.4 %all_gather.21 = bf16[256,1536]{1,0:T(8,128)(2,1)S(1)} all-gather(bf16[16,1536]{1,0:T(8,128)(2,1)S(1)} %get-tuple-element.22), channel_id=1, replica_groups=mesh['fs'=16,'tp'=2] {'fs'}, dimensions={0}, use_global_device_ids=true | all-gather | bytes 835584 | tf_op jit(solution)/shard_map/all_gather | solution.py:53
  402.7 0.7 slice.44
  403.4 0.7 slice.45
  404.3 0.6 slice.48
  405.6 0.6 slice.49
  406.8 1.0 copy.23
  407.8 1.0 copy.25
  408.8 0.8 copy.22
  409.6 0.8 copy.24
  410.5 52.2 %all-gather.8.cloned.1.call-done = bf16[2048,512]{0,1:T(8,128)(2,1)} async-done(((bf16[128,512]{0,1:T(8,128)(2,1)}), bf16[2048,512]{0,1:T(8,128)(2,1)}) %all-gather.8.cloned.1.call-update) | async-done | bytes 2097168 | tf_op jit(solution)/shard_map/all_gather | solution.py:59
  462.7 3.9 copy.26
  466.6 86.1 %all-gather.10.cloned.1.call-done = bf16[2048,1024]{0,1:T(8,128)(2,1)} async-done(((bf16[128,1024]{0,1:T(8,128)(2,1)}), bf16[2048,1024]{0,1:T(8,128)(2,1)}) %all-gather.10.cloned.1.call-update) | async-done | bytes 4194320 | tf_op jit(solution)/shard_map/all_gather | solution.py:60
  552.7 6.4 %copy.27 = bf16[2048,1024]{1,0:T(8,128)(2,1)} copy(bf16[2048,1024]{0,1:T(8,128)(2,1)} %all-gather.10.cloned.1.call-done) | data formatting | bytes 8388608
  (31 shorter events, 2.8 us)
Async XLA Ops:
  7.2 61.4 %all-gather.6.cloned.1.call-start = ((), (), s32[]{:S(2)}) async-start(), calls=%async_computation | async-start | bytes 1114112 | tf_op jit(solution)/shard_map/all_gather | solution.py:31
  7.9 337.1 %all-gather.12.cloned.1.call-start = ((), (), s32[]{:S(2)}) async-start(), calls=%async_computation.3 | async-start | bytes 26738688 | tf_op jit(solution)/shard_map/all_gather | solution.py:42
  8.0 1.9 copy-start
  73.4 3.5 copy-start.2
  75.6 387.1 %all-gather.8.cloned.1.call-start = ((), (), s32[]{:S(2)}) async-start(), calls=%async_computation.1 | async-start | bytes 2228224 | tf_op jit(solution)/shard_map/all_gather | solution.py:59
  345.0 14.7 %copy-start.3 = (f32[16,1024]{1,0:T(8,128)S(1)}, f32[16,1024]{1,0:T(8,128)}, u32[]{:S(2)}) copy-start(f32[16,1024]{1,0:T(8,128)} %param.19) | copy-start | bytes 196612
  345.1 14.7 %copy-start.4 = (f32[16,1024]{1,0:T(8,128)S(1)}, f32[16,1024]{1,0:T(8,128)}, u32[]{:S(2)}) copy-start(f32[16,1024]{1,0:T(8,128)} %param.18) | copy-start | bytes 196612
  345.1 14.7 %copy-start.5 = (f32[16,512]{1,0:T(8,128)S(1)}, f32[16,512]{1,0:T(8,128)}, u32[]{:S(2)}) copy-start(f32[16,512]{1,0:T(8,128)} %param.17) | copy-start | bytes 98308
  345.1 14.8 %copy-start.6 = (f32[16,512]{1,0:T(8,128)S(1)}, f32[16,512]{1,0:T(8,128)}, u32[]{:S(2)}) copy-start(f32[16,512]{1,0:T(8,128)} %param.16) | copy-start | bytes 98308
  345.1 57.2 %copy-start.1 = (bf16[128,256]{1,0:T(8,128)(2,1)S(1)}, bf16[128,256]{1,0:T(8,128)(2,1)}, u32[]{:S(2)}) copy-start(bf16[128,256]{1,0:T(8,128)(2,1)} %param.13) | copy-start | bytes 196612
  403.4 149.4 %all-gather.10.cloned.1.call-start = ((), (), s32[]{:S(2)}) async-start(), calls=%async_computation.2 | async-start | bytes 4456448 | tf_op jit(solution)/shard_map/all_gather | solution.py:60
Sparse Core Ops, SparseCore 0:
  10.7 57.7 all-gather.5
  75.7 269.3 all-gather.11
  403.5 59.1 all-gather.7
  465.8 86.8 all-gather.9
